TPU v7x, 32 devices: a whole 2x2x4 slice. The times are simulated.
32 devices in a mesh: sp: 8 (over z, x), tp: 4 (over y, core).
Axes of the slice: x: 2, y: 2, z: 4, core: 2. Of those that a mesh axis runs over, the one named last changes fastest.
Arguments:
- queries: bfloat16 [1024, 32, 128], P('sp', 'tp'), may hold values from -6 to 6
- keys: bfloat16 [1024, 8, 128], P('sp', 'tp'), may hold values from -6 to 6
- values: bfloat16 [1024, 8, 128], P('sp', 'tp'), may hold values from -6 to 6
- q_gain: float32 [128], replicated, may hold values from 0.2 to 8
- k_gain: float32 [128], replicated, may hold values from 0.2 to 8
- w_out: bfloat16 [4096, 2048], P('tp'), may hold values from -0.09375 to 0.09375
- residual: bfloat16 [1024, 2048], P(('sp', 'tp')), may hold values from -6 to 6
- gain_mix: float32 [2048], replicated, may hold values from 0.1 to 1.9
- gain_pre: float32 [2048], replicated, may hold values from 0.1 to 1.9
- routes: int32 [1024, 4], P(('sp', 'tp')), may hold values from 0 to 7, all different within a row; in each aligned block of 32 rows (0 to 31, 32 to 63, ...) at most 32 rows name the same one
- route_weights: float32 [1024, 4], P(('sp', 'tp')), may hold values from 0.1 to 1
- w_gate: bfloat16 [8, 2048, 2048], P('sp', None, 'tp'), may hold values from -0.5 to 0.5
- w_up: bfloat16 [8, 2048, 2048], P('sp', None, 'tp'), may hold values from -0.5 to 0.5
- w_down: bfloat16 [8, 2048, 2048], P('sp', 'tp'), may hold values from -0.125 to 0.125
- gain_moe: float32 [2048], replicated, may hold values from 0.1 to 1.9
Outputs:
- layer_out: bfloat16 [1024, 2048], P(('sp', 'tp'))
Inputs may be any that keep to these rules, and one draw needn't show every extreme that they name: `routes`: each row names 4 different experts. In each aligned block of 32 rows (the rows of one device) no expert is named by more than 32 rows, a bound that some block reaches.
All inputs are finite; a program needn't handle non-finite values.
Results may differ from a plain program's by a relative error of at most 0.017.
The roundings to bfloat16 on the way count: a program that leaves them out, or rounds other values in their place, can miss the bound.
Values may be sent and summed in bfloat16 or wider, within the bound.
No kernel may reach another device: no remote copies, remote signals or barrier semaphores. Data moves between devices by JAX's collectives and lax.ppermute only.
A program may use at most 128 MiB of HBM per device.

v0:
```python
import math
import jax
import jax.numpy as jnp
from jax import lax
from jax.sharding import PartitionSpec as P

TOP = 4
GRID_W = 64
norm_eps = 1e-06
rope_theta = 10000.0
clamp_limit = 7.0
swish_alpha = 1.702


def rope_tables(positions, head_size):
    row_index = (positions // GRID_W).astype(jnp.float32)
    col_index = (positions % GRID_W).astype(jnp.float32)
    freq_count = head_size // 4
    inverse = rope_theta ** (-jnp.arange(freq_count, dtype=jnp.float32) / freq_count)
    angles = jnp.stack([row_index[:, None] * inverse, col_index[:, None] * inverse], axis=1)
    return (jnp.cos(angles), jnp.sin(angles))


def turn(array_in, cosine_table, sine_table):
    token_count, head_count, head_size = array_in.shape
    split_field = array_in.reshape(token_count, head_count, 2, 2, head_size // 4)
    first_half = split_field[:, :, :, 0, :]
    second_half = split_field[:, :, :, 1, :]
    cos_wide = cosine_table[:, None]
    sin_wide = sine_table[:, None]
    turned = jnp.stack(
        [
            first_half * cos_wide - second_half * sin_wide,
            second_half * cos_wide + first_half * sin_wide,
        ],
        axis=3,
    )
    return turned.reshape(token_count, head_count, head_size)


def scale_rows(array_in, gain_vec):
    return (
        array_in
        * lax.rsqrt(jnp.mean(array_in * array_in, axis=-1, keepdims=True) + norm_eps)
        * gain_vec
    )


def slot_table(route_rows, experts, capacity):
    flat_routes = route_rows.reshape(-1)
    expert_hits = (flat_routes[:, None] == jnp.arange(experts, dtype=jnp.int32)[None, :]).astype(
        jnp.int32
    )
    slot_index = jnp.sum((jnp.cumsum(expert_hits, axis=0) - expert_hits) * expert_hits, axis=1)
    target = flat_routes * capacity + slot_index
    slot_onehot = target[:, None] == jnp.arange(experts * capacity, dtype=jnp.int32)[None, :]
    return slot_onehot.astype(jnp.bfloat16).reshape(
        route_rows.shape[0], route_rows.shape[1], experts * capacity
    )


def expert_apply(arrived_rows, w_gate, w_up, w_down):
    gate_pre = jnp.minimum(
        jnp.einsum("serd,edf->serf", arrived_rows, w_gate, preferred_element_type=jnp.float32),
        clamp_limit,
    )
    up_pre = jnp.clip(
        jnp.einsum("serd,edf->serf", arrived_rows, w_up, preferred_element_type=jnp.float32),
        -clamp_limit,
        clamp_limit,
    )
    active = (gate_pre * jax.nn.sigmoid(swish_alpha * gate_pre) * (up_pre + 1.0)).astype(
        jnp.bfloat16
    )
    partial_value = jnp.einsum("serf,efd->serd", active, w_down, preferred_element_type=jnp.float32)
    return lax.optimization_barrier(partial_value.astype(jnp.bfloat16)).astype(jnp.float32)


def send_back(finished):
    return lax.all_to_all(finished, "sp", split_axis=0, concat_axis=0, tiled=True)


def on_device(
    queries,
    keys,
    values,
    q_gain,
    k_gain,
    w_out,
    residual,
    gain_mix,
    gain_pre,
    routes,
    route_weights,
    w_gate,
    w_up,
    w_down,
    gain_moe,
):
    tok_rows, head_local, head_size = queries.shape
    kv_local = keys.shape[1]
    group_size = head_local // kv_local
    positions = lax.axis_index("sp") * tok_rows + jnp.arange(tok_rows, dtype=jnp.int32)
    cosine_table, sine_table = rope_tables(positions, head_size)
    q_turned = (
        turn(scale_rows(queries.astype(jnp.float32), q_gain), cosine_table, sine_table)
        * head_size ** (-0.5)
    ).astype(jnp.bfloat16)
    k_turned = turn(scale_rows(keys.astype(jnp.float32), k_gain), cosine_table, sine_table).astype(
        jnp.bfloat16
    )
    q_grouped = q_turned.reshape(tok_rows, kv_local, group_size, head_size)
    initial = (
        jnp.full((kv_local, group_size, tok_rows), -jnp.inf, jnp.float32),
        jnp.zeros((kv_local, group_size, tok_rows), jnp.float32),
        jnp.zeros((kv_local, group_size, tok_rows, head_size), jnp.float32),
    )
    carry_state = initial
    key_piece = lax.all_gather(k_turned, "sp", axis=0, tiled=True)
    value_piece = lax.all_gather(values, "sp", axis=0, tiled=True)
    piece_rows = key_piece.shape[0]
    block_rows = math.gcd(piece_rows, 1024)
    key_blocks = key_piece.reshape(piece_rows // block_rows, block_rows, kv_local, head_size)
    value_blocks = value_piece.reshape(piece_rows // block_rows, block_rows, kv_local, head_size)

    def absorb_block(state_now, key_value):
        running_max, running_sum, weighted = state_now
        key_block, value_block = key_value
        scores = jnp.einsum(
            "qkgd,skd->kgqs", q_grouped, key_block, preferred_element_type=jnp.float32
        )
        new_max = jnp.maximum(running_max, jnp.max(scores, axis=-1))
        rescale = jnp.exp(running_max - new_max)
        unnorm = jnp.exp(scores - new_max[..., None])
        running_sum = running_sum * rescale + jnp.sum(unnorm, axis=-1)
        weighted = weighted * rescale[..., None] + jnp.einsum(
            "kgqs,skd->kgqd",
            unnorm.astype(jnp.bfloat16),
            value_block,
            preferred_element_type=jnp.float32,
        )
        return ((new_max, running_sum, weighted), None)

    carry_state, ignored = lax.scan(absorb_block, carry_state, (key_blocks, value_blocks))
    running_max, running_sum, weighted = carry_state
    mixed_heads = (weighted / running_sum[..., None]).transpose(2, 0, 1, 3)
    mixed_heads = mixed_heads.reshape(tok_rows, head_local * head_size).astype(jnp.bfloat16)
    tok_part = residual.shape[0]
    width = residual.shape[1]
    projected = lax.psum_scatter(
        jnp.dot(mixed_heads, w_out, preferred_element_type=jnp.float32).astype(jnp.bfloat16),
        "tp",
        scatter_dimension=0,
        tiled=True,
    ).astype(jnp.float32)
    middle = residual.astype(jnp.float32) + scale_rows(projected, gain_mix)
    normed = scale_rows(middle, gain_pre).astype(jnp.bfloat16)
    local_experts = w_gate.shape[0]
    experts_all = local_experts * lax.axis_size("sp")
    capacity = max(2, (2 * tok_part * TOP + experts_all - 1) // experts_all)
    tables = slot_table(routes, experts_all, capacity)
    chosen = jnp.sum(tables, axis=1)
    outbound = jnp.einsum("tp,td->pd", chosen, normed, preferred_element_type=jnp.float32)
    outbound = outbound.astype(jnp.bfloat16).reshape(experts_all, capacity, width)
    arrived_rows = lax.all_gather(
        lax.all_to_all(outbound, "sp", split_axis=0, concat_axis=0, tiled=True),
        "tp",
        axis=0,
        tiled=True,
    )
    leading = arrived_rows.shape[0] // local_experts
    partial_value = expert_apply(
        arrived_rows.reshape(leading, local_experts, arrived_rows.shape[1], width),
        w_gate,
        w_up,
        w_down,
    )
    summed = lax.psum_scatter(
        partial_value.reshape(arrived_rows.shape).astype(jnp.bfloat16),
        "tp",
        scatter_dimension=0,
        tiled=True,
    )
    returned = send_back(summed)
    gathered = jnp.einsum(
        "tkp,pd->tkd",
        tables,
        returned.reshape(experts_all * capacity, width),
        preferred_element_type=jnp.float32,
    )
    mixture = jnp.sum(gathered * route_weights[:, :, None], axis=1)
    return (middle + scale_rows(mixture, gain_moe)).astype(jnp.bfloat16)


def solution(mesh):
    placed = (
        P("sp", "tp", None),
        P("sp", "tp", None),
        P("sp", "tp", None),
        P(),
        P(),
        P("tp", None),
        P(("sp", "tp"), None),
        P(),
        P(),
        P(("sp", "tp"), None),
        P(("sp", "tp"), None),
        P("sp", None, "tp"),
        P("sp", None, "tp"),
        P("sp", "tp", None),
        P(),
    )
    return jax.shard_map(
        on_device, mesh=mesh, in_specs=placed, out_specs=P(("sp", "tp"), None), check_vma=False
    )
```

profile of v0, /device:TPU:0, one launch (start us, length us, event | category | flops | bytes accessed | tf_op | source)
XLA Modules:
  0.0 267.1 jit_solution(2984971475194426291)
XLA Ops:
  6.6 1.1 copy.57
  7.9 0.7 fusion.46
  8.9 1.0 copy.61
  9.8 1.2 copy.59
  11.1 0.8 fusion.37
  11.9 29.6 %all_gather.10 = bf16[1024,2,128]{0,2,1:T(8,128)(2,1)S(1)} all-gather(bf16[128,2,128]{0,2,1:T(8,128)(2,1)S(1)} %copy.61), channel_id=1, replica_groups=mesh['sp'=8,'tp'=4] {'sp'}, dimensions={0}, use_global_device_ids=true | all-gather | bytes 589824 | tf_op jit(solution)/shard_map/all_gather | solution.py:120
  41.5 31.4 %all_gather.9 = bf16[1024,2,128]{2,0,1:T(8,128)(2,1)S(1)} all-gather(bf16[128,2,128]{2,0,1:T(8,128)(2,1)S(1)} %copy.58), channel_id=1, replica_groups=mesh['sp'=8,'tp'=4] {'sp'}, dimensions={0}, use_global_device_ids=true | all-gather | bytes 589824 | tf_op jit(solution)/shard_map/all_gather | solution.py:119
  73.0 0.7 bitcast_reduce_fusion
  73.7 0.6 fusion.1
  74.3 0.9 fusion.31
  75.2 1.3 copy-done.1
  76.5 1.5 convolution_convert_fusion.1
  79.1 20.0 %reduce-scatter.3.cloned.1.call-done = bf16[32,2048]{1,0:T(8,128)(2,1)} async-done(((bf16[128,2048]{1,0:T(8,128)(2,1)}), bf16[32,2048]{1,0:T(8,128)(2,1)}) %reduce-scatter.3.cloned.1.call-update) | async-done | bytes 131088 | tf_op jit(solution)/shard_map/reduce_scatter | solution.py:150
  99.1 1.0 fusion.42
  100.2 1.1 multiply_reduce_fusion.1
  101.4 1.4 convolution_convert_fusion
  102.8 31.0 %all_to_all.10 = bf16[8,32,2048]{2,1,0:T(8,128)(2,1)} all-to-all(bf16[8,32,2048]{2,1,0:T(8,128)(2,1)S(1)} %bitcast.129), channel_id=1, replica_groups=mesh['sp'=8,'tp'=4] {'sp'}, dimensions={0} | all-to-all | bytes 2097152 | tf_op jit(solution)/shard_map/all_to_all | solution.py:166
  133.8 32.6 %all-gather.2.cloned.1.call-done = bf16[32,32,2048]{2,1,0:T(8,128)(2,1)} async-done(((bf16[8,32,2048]{2,1,0:T(8,128)(2,1)}), bf16[32,32,2048]{2,1,0:T(8,128)(2,1)}) %all-gather.2.cloned.1.call-update) | async-done | bytes 4194320 | tf_op jit(solution)/shard_map/all_gather | solution.py:165
  166.5 6.6 %fusion.7 = f32[32,32,512]{2,1,0:T(8,128)} fusion(bf16[32,32,2048]{2,1,0:T(8,128)(2,1)} %all-gather.2.cloned.1.call-done, bf16[1,2048,512]{2,1,0:T(8,128)(2,1)} %param.27), kind=kOutput, calls=%fused_computation.13 | convolution fusion | flops 2147483648 | bytes 8388608 | tf_op jit(solution)/shard_map/serd,edf->serf/dot_general | solution.py:68
  173.1 10.3 %convert_bitcast_fusion = bf16[32,1,32,2048]{3,2,0,1:T(8,128)(2,1)} fusion(bf16[1,512,2048]{2,1,0:T(8,128)(2,1)S(1)} %copy-done, f32[32,32,512]{2,1,0:T(8,128)} %fusion.7, bf16[32,32,2048]{2,1,0:T(8,128)(2,1)} %all-gather.2.cloned.1.call-done, bf16[1,2048,512]{2,1,0:T(8,128)(2,1)} %param.26), kind=kOutput, calls=%fused_computation.3 | convolution fusion | flops 4302307328 | bytes 14680064 | tf_op jit(solution)/shard_map/serf,efd->serd/dot_general | solution.py:75
  183.4 44.7 %reduce-scatter.5.cloned.1.call-done = bf16[8,32,2048]{2,1,0:T(8,128)(2,1)} async-done(((bf16[32,32,2048]{2,1,0:T(8,128)(2,1)}), bf16[8,32,2048]{2,1,0:T(8,128)(2,1)}) %reduce-scatter.5.cloned.1.call-update) | async-done | bytes 1048592 | tf_op jit(solution)/shard_map/reduce_scatter | solution.py:178
  228.1 31.1 %all_to_all.11 = bf16[8,32,2048]{2,1,0:T(8,128)(2,1)S(1)} all-to-all(bf16[8,32,2048]{2,1,0:T(8,128)(2,1)} %reduce-scatter.5.cloned.1.call-done), channel_id=1, replica_groups=mesh['sp'=8,'tp'=4] {'sp'}, dimensions={0} | all-to-all | bytes 2097152 | tf_op jit(solution)/shard_map/all_to_all | solution.py:80
  259.2 0.3 fusion.21
  259.8 0.8 add_convert_fusion
  (51 shorter events, 1.9 us)
Async XLA Ops:
  6.5 166.5 %copy-start = (bf16[1,512,2048]{2,1,0:T(8,128)(2,1)S(1)}, bf16[1,512,2048]{2,1,0:T(8,128)(2,1)}, u32[]{:S(2)}) copy-start(bf16[1,512,2048]{2,1,0:T(8,128)(2,1)} %param.28) | copy-start | bytes 6291460
  6.5 92.6 %reduce-scatter.3.cloned.1.call-start = ((), (), s32[]{:S(2)}) async-start(), calls=%async_computation.4 | async-start | bytes 655360 | tf_op jit(solution)/shard_map/reduce_scatter | solution.py:150
  74.3 2.2 copy-start.1
  76.5 1.6 copy-start.7
  76.5 23.6 %copy-start.3 = (bf16[32,2048]{1,0:T(8,128)(2,1)S(1)}, bf16[32,2048]{1,0:T(8,128)(2,1)}, u32[]{:S(2)}) copy-start(bf16[32,2048]{1,0:T(8,128)(2,1)} %param.21) | copy-start | bytes 393220
  76.5 23.7 %copy-start.4 = (f32[2048]{0:T(1024)S(1)}, f32[2048]{0:T(1024)}, u32[]{:S(2)}) copy-start(f32[2048]{0:T(1024)} %param.22) | copy-start | bytes 24580
  76.5 24.8 %copy-start.5 = (f32[2048]{0:T(1024)S(1)}, f32[2048]{0:T(1024)}, u32[]{:S(2)}) copy-start(f32[2048]{0:T(1024)} %param.23) | copy-start | bytes 24580
  78.1 88.4 %all-gather.2.cloned.1.call-start = ((), (), s32[]{:S(2)}) async-start(), calls=%async_computation.5 | async-start | bytes 5242880 | tf_op jit(solution)/shard_map/all_gather | solution.py:165
  133.8 94.3 %reduce-scatter.5.cloned.1.call-start = ((), (), s32[]{:S(2)}) async-start(), calls=%async_computation.6 | async-start | bytes 5242880 | tf_op jit(solution)/shard_map/reduce_scatter | solution.py:178
  183.4 75.8 %copy-start.8 = (f32[32,4]{0,1:T(4,128)S(1)}, f32[32,4]{0,1:T(4,128)}, u32[]{:S(2)}) copy-start(f32[32,4]{0,1:T(4,128)} %param.25) | copy-start | bytes 1540
  183.4 76.3 %copy-start.2 = (bf16[32,2048]{1,0:T(8,128)(2,1)S(1)}, bf16[32,2048]{1,0:T(8,128)(2,1)}, u32[]{:S(2)}) copy-start(bf16[32,2048]{1,0:T(8,128)(2,1)} %reduce-scatter.3.cloned.1.call-done) | copy-start | bytes 393220
  183.4 76.3 %copy-start.6 = (f32[2048]{0:T(1024)S(1)}, f32[2048]{0:T(1024)}, u32[]{:S(2)}) copy-start(f32[2048]{0:T(1024)} %param.29) | copy-start | bytes 24580
Sparse Core Ops, SparseCore 0:
  78.2 20.8 reduce-scatter.2
  133.9 32.5 all-gather.1
  183.5 44.5 reduce-scatter.4
where the time goes:
time: 268 us; the launch traced here: 267 us
  blocking collectives  123 us (46%)
  waiting for transfers between devices  97.4 us (36%)
  matrix products  21.8 us (8%)
  between operations  13.4 us (5%)
  other arithmetic  6.28 us (2%)
  local copies, waits for them, and re-layouts  5.04 us (2%)
    reduce_scatter x1, waiting for transfers between devices, on_device(): lax.psum_scatter(partial_value.reshape(arrived_rows.shape).astype(jnp.bfl...  44.7 us
    all_gather x1, waiting for transfers between devices, on_device(): lax.all_gather(lax.all_to_all(outbound, 'sp', split_axis=0, concat_axis=0...  32.6 us
    all_gather x1, blocking collectives, on_device(): key_piece = lax.all_gather(k_turned, 'sp', axis=0, tiled=True)  31.4 us
    all_to_all x1, blocking collectives, send_back(): lax.all_to_all(finished, 'sp', split_axis=0, concat_axis=0, tiled=True)  31.1 us
    all_to_all x1, blocking collectives, on_device(): lax.all_to_all(outbound, 'sp', split_axis=0, concat_axis=0, tiled=True)  31 us
    all_gather x1, blocking collectives, on_device(): value_piece = lax.all_gather(values, 'sp', axis=0, tiled=True)  29.6 us
    reduce_scatter x1, waiting for transfers between devices, on_device(): lax.psum_scatter(jnp.dot(mixed_heads, w_out, preferred_element_type=jnp.f...  20 us
    dot_general x1, matrix products, expert_apply(): jnp.einsum('serf,efd->serd', active, w_down, preferred_element_type=jnp.f...  10.3 us
  transfers between devices with their start and end apart: 3, of which 3 were waited for; matrix products, arithmetic and copies ran while one was open for 0% of the time, Pallas kernels for 0%

commit v1 on v0

--- a/solution.py
+++ b/solution.py
@@ -10,6 +10,12 @@
 rope_theta = 10000.0
 clamp_limit = 7.0
 swish_alpha = 1.702
+
+
+def replace_scales_now(t0, field):
+    e_next = jnp.concatenate([t0, field], axis=1)
+    reached = jax.lax.all_gather(e_next, axis_name="sp", axis=0, tiled=True)
+    return jnp.split(reached, [t0.shape[1]], axis=1)
 
 
 def rope_tables(positions, head_size):
@@ -116,8 +122,7 @@
         jnp.zeros((kv_local, group_size, tok_rows, head_size), jnp.float32),
     )
     carry_state = initial
-    key_piece = lax.all_gather(k_turned, "sp", axis=0, tiled=True)
-    value_piece = lax.all_gather(values, "sp", axis=0, tiled=True)
+    key_piece, value_piece = replace_scales_now(k_turned, values)
     piece_rows = key_piece.shape[0]
     block_rows = math.gcd(piece_rows, 1024)
     key_blocks = key_piece.reshape(piece_rows // block_rows, block_rows, kv_local, head_size)

time: 268 us -> 249 us (0.929)
  blocking collectives: 123 us -> 62.1 us
  waiting for transfers between devices: 97.4 us -> 139 us
    all_gather x2 -> x0, blocking collectives: 61 us -> none  [the longest x1 31.4 us: on_device(): key_piece = lax.all_gather(k_turned, 'sp', axis=0, tiled=True)]
    all_gather x0 -> x1, waiting for transfers between devices: none -> 41.6 us  [replace_scales_now(): reached = jax.lax.all_gather(e_next, axis_name='sp', axis=0, tiled=True)]
  transfers between devices with their start and end apart: 3 -> 4, of which waited for: 3 -> 4; matrix products, arithmetic and copies ran while one was open for 0% -> 1% of each run, Pallas kernels for 0% -> 0%
where the time goes in v1:
time: 249 us
  waiting for transfers between devices  139 us (56%)
  blocking collectives  62.1 us (25%)
  matrix products  22.7 us (9%)
  between operations  13.4 us (5%)
  other arithmetic  6.28 us (3%)
  local copies, waits for them, and re-layouts  5.7 us (2%)
    reduce_scatter x1, waiting for transfers between devices, on_device(): lax.psum_scatter(partial_value.reshape(arrived_rows.shape).astype(jnp.bfl...  44.7 us
    all_gather x1, waiting for transfers between devices, replace_scales_now(): reached = jax.lax.all_gather(e_next, axis_name='sp', axis=0, tiled=True)  41.6 us
    all_gather x1, waiting for transfers between devices, on_device(): lax.all_gather(lax.all_to_all(outbound, 'sp', split_axis=0, concat_axis=0...  32.6 us
    all_to_all x1, blocking collectives, send_back(): lax.all_to_all(finished, 'sp', split_axis=0, concat_axis=0, tiled=True)  31.1 us
    all_to_all x1, blocking collectives, on_device(): lax.all_to_all(outbound, 'sp', split_axis=0, concat_axis=0, tiled=True)  31 us
    reduce_scatter x1, waiting for transfers between devices, on_device(): lax.psum_scatter(jnp.dot(mixed_heads, w_out, preferred_element_type=jnp.f...  19.5 us
    dot_general x1, matrix products, expert_apply(): jnp.einsum('serf,efd->serd', active, w_down, preferred_element_type=jnp.f...  10.3 us
    dot_general x1, matrix products, expert_apply(): jnp.einsum('serd,edf->serf', arrived_rows, w_up, preferred_element_type=j...  6.59 us
  transfers between devices with their start and end apart: 4, of which 4 were waited for; matrix products, arithmetic and copies ran while one was open for 1% of the time, Pallas kernels for 0%

profile of v1, /device:TPU:0, one launch (start us, length us, event | category | flops | bytes accessed | tf_op | source)
XLA Modules:
  0.0 248.9 jit_solution(15564540216927653685)
XLA Ops:
  6.6 1.1 copy.61
  7.9 0.7 fusion.44
  8.9 0.9 copy.63
  9.7 0.7 pad_maximum_fusion
  10.5 1.2 copy.64
  12.0 41.6 %all-gather.3.cloned.1.call-done = bf16[1024,4,128]{2,0,1:T(8,128)(2,1)} async-done(((bf16[128,4,128]{2,0,1:T(8,128)(2,1)}), bf16[1024,4,128]{2,0,1:T(8,128)(2,1)}) %all-gather.3.cloned.1.call-update) | async-done | bytes 1048592 | tf_op jit(solution)/shard_map/all_gather | solution.py:17
  53.6 1.7 bitcast_reduce_fusion
  55.3 0.6 fusion.1
  55.9 0.6 copy-done.4
  56.5 0.8 fusion.31
  57.3 1.4 copy-done.1
  58.7 1.5 convolution_convert_fusion.1
  61.3 19.5 %reduce-scatter.3.cloned.1.call-done = bf16[32,2048]{1,0:T(8,128)(2,1)} async-done(((bf16[128,2048]{1,0:T(8,128)(2,1)}), bf16[32,2048]{1,0:T(8,128)(2,1)}) %reduce-scatter.3.cloned.1.call-update) | async-done | bytes 131088 | tf_op jit(solution)/shard_map/reduce_scatter | solution.py:155
  80.9 1.0 fusion.40
  81.9 1.1 multiply_reduce_fusion.1
  83.1 1.4 convolution_convert_fusion
  84.5 31.0 %all_to_all.10 = bf16[8,32,2048]{2,1,0:T(8,128)(2,1)} all-to-all(bf16[8,32,2048]{2,1,0:T(8,128)(2,1)S(1)} %bitcast.129), channel_id=1, replica_groups=mesh['sp'=8,'tp'=4] {'sp'}, dimensions={0} | all-to-all | bytes 2097152 | tf_op jit(solution)/shard_map/all_to_all | solution.py:171
  115.6 32.6 %all-gather.5.cloned.1.call-done = bf16[32,32,2048]{2,1,0:T(8,128)(2,1)} async-done(((bf16[8,32,2048]{2,1,0:T(8,128)(2,1)}), bf16[32,32,2048]{2,1,0:T(8,128)(2,1)}) %all-gather.5.cloned.1.call-update) | async-done | bytes 4194320 | tf_op jit(solution)/shard_map/all_gather | solution.py:170
  148.2 6.6 %fusion.7 = f32[32,32,512]{2,1,0:T(8,128)} fusion(bf16[32,32,2048]{2,1,0:T(8,128)(2,1)} %all-gather.5.cloned.1.call-done, bf16[1,2048,512]{2,1,0:T(8,128)(2,1)} %param.27), kind=kOutput, calls=%fused_computation.13 | convolution fusion | flops 2147483648 | bytes 8388608 | tf_op jit(solution)/shard_map/serd,edf->serf/dot_general | solution.py:74
  154.8 10.3 %convert_bitcast_fusion = bf16[32,1,32,2048]{3,2,0,1:T(8,128)(2,1)} fusion(bf16[1,512,2048]{2,1,0:T(8,128)(2,1)S(1)} %copy-done, f32[32,32,512]{2,1,0:T(8,128)} %fusion.7, bf16[32,32,2048]{2,1,0:T(8,128)(2,1)} %all-gather.5.cloned.1.call-done, bf16[1,2048,512]{2,1,0:T(8,128)(2,1)} %param.26), kind=kOutput, calls=%fused_computation.3 | convolution fusion | flops 4302307328 | bytes 14680064 | tf_op jit(solution)/shard_map/serf,efd->serd/dot_general | solution.py:81
  165.2 44.7 %reduce-scatter.5.cloned.1.call-done = bf16[8,32,2048]{2,1,0:T(8,128)(2,1)} async-done(((bf16[32,32,2048]{2,1,0:T(8,128)(2,1)}), bf16[8,32,2048]{2,1,0:T(8,128)(2,1)}) %reduce-scatter.5.cloned.1.call-update) | async-done | bytes 1048592 | tf_op jit(solution)/shard_map/reduce_scatter | solution.py:183
  209.9 31.1 %all_to_all.11 = bf16[8,32,2048]{2,1,0:T(8,128)(2,1)S(1)} all-to-all(bf16[8,32,2048]{2,1,0:T(8,128)(2,1)} %reduce-scatter.5.cloned.1.call-done), channel_id=1, replica_groups=mesh['sp'=8,'tp'=4] {'sp'}, dimensions={0} | all-to-all | bytes 2097152 | tf_op jit(solution)/shard_map/all_to_all | solution.py:86
  241.0 0.3 fusion.21
  241.5 0.8 add_convert_fusion
  (57 shorter events, 2.1 us)
Async XLA Ops:
  6.5 148.3 %copy-start = (bf16[1,512,2048]{2,1,0:T(8,128)(2,1)S(1)}, bf16[1,512,2048]{2,1,0:T(8,128)(2,1)}, u32[]{:S(2)}) copy-start(bf16[1,512,2048]{2,1,0:T(8,128)(2,1)} %param.28) | copy-start | bytes 6291460
  6.5 5.2 %copy-start.10 = (f32[128]{0:T(128)S(1)}, f32[128]{0:T(128)}, u32[]{:S(2)}) copy-start(f32[128]{0:T(128)} %param.18) | copy-start | bytes 1540
  6.5 47.0 %all-gather.3.cloned.1.call-start = ((), (), s32[]{:S(2)}) async-start(), calls=%async_computation.4 | async-start | bytes 1179648 | tf_op jit(solution)/shard_map/all_gather | solution.py:17
  10.4 70.4 %reduce-scatter.3.cloned.1.call-start = ((), (), s32[]{:S(2)}) async-start(), calls=%async_computation.5 | async-start | bytes 655360 | tf_op jit(solution)/shard_map/reduce_scatter | solution.py:155
  55.3 1.2 copy-start.4
  56.5 2.2 copy-start.1
  58.7 1.6 copy-start.8
  58.7 23.2 %copy-start.3 = (bf16[32,2048]{1,0:T(8,128)(2,1)S(1)}, bf16[32,2048]{1,0:T(8,128)(2,1)}, u32[]{:S(2)}) copy-start(bf16[32,2048]{1,0:T(8,128)(2,1)} %param.21) | copy-start | bytes 393220
  58.7 23.2 %copy-start.5 = (f32[2048]{0:T(1024)S(1)}, f32[2048]{0:T(1024)}, u32[]{:S(2)}) copy-start(f32[2048]{0:T(1024)} %param.22) | copy-start | bytes 24580
  58.7 24.3 %copy-start.6 = (f32[2048]{0:T(1024)S(1)}, f32[2048]{0:T(1024)}, u32[]{:S(2)}) copy-start(f32[2048]{0:T(1024)} %param.23) | copy-start | bytes 24580
  60.3 87.9 %all-gather.5.cloned.1.call-start = ((), (), s32[]{:S(2)}) async-start(), calls=%async_computation.6 | async-start | bytes 5242880 | tf_op jit(solution)/shard_map/all_gather | solution.py:170
  115.5 94.3 %reduce-scatter.5.cloned.1.call-start = ((), (), s32[]{:S(2)}) async-start(), calls=%async_computation.7 | async-start | bytes 5242880 | tf_op jit(solution)/shard_map/reduce_scatter | solution.py:183
  165.2 75.8 %copy-start.9 = (f32[32,4]{0,1:T(4,128)S(1)}, f32[32,4]{0,1:T(4,128)}, u32[]{:S(2)}) copy-start(f32[32,4]{0,1:T(4,128)} %param.25) | copy-start | bytes 1540
  165.2 76.3 %copy-start.2 = (bf16[32,2048]{1,0:T(8,128)(2,1)S(1)}, bf16[32,2048]{1,0:T(8,128)(2,1)}, u32[]{:S(2)}) copy-start(bf16[32,2048]{1,0:T(8,128)(2,1)} %reduce-scatter.3.cloned.1.call-done) | copy-start | bytes 393220
  165.2 76.3 %copy-start.7 = (f32[2048]{0:T(1024)S(1)}, f32[2048]{0:T(1024)}, u32[]{:S(2)}) copy-start(f32[2048]{0:T(1024)} %param.29) | copy-start | bytes 24580
Sparse Core Ops, SparseCore 0:
  10.5 42.9 all-gather.2
  60.4 20.3 reduce-scatter.2
  115.7 32.5 all-gather.4
  165.3 44.5 reduce-scatter.4
